TPU v7x, 32 devices: a whole 2x2x4 slice. The times are simulated.
32 devices in a mesh: fs: 4 (over z), rep: 4 (over y, x), tp: 2 (over core).
Axes of the slice: x: 2, y: 2, z: 4, core: 2. Of those that a mesh axis runs over, the one named last changes fastest.
Arguments:
- saved_input: bfloat16 [16384, 2048], P(('fs', 'rep')), may hold values from -6 to 6
- value_cotangent: bfloat16 [16384, 4096], P(('fs', 'rep'), 'tp'), may hold values from -0.0061950684 to 0.0061950684
- factor: bfloat16 [2048, 128], P('fs'), may hold values from -1.5 to 1.5
- weight: float32 [2048, 4096], P('fs', 'tp'), may hold values from -1.2 to 1.2
- first_moment: float32 [128, 4096], P('fs', 'tp'), may hold values from -1.8 to 1.8
- second_moment: float32 [128, 4096], P('fs', 'tp'), may hold values from 0.1 to 1
Outputs:
- low_grad: float32 [128, 4096], P('fs', 'tp')
- new_first: float32 [128, 4096], P('fs', 'tp')
- new_second: float32 [128, 4096], P('fs', 'tp')
- direction: float32 [2048, 4096], P('fs', 'tp')
- new_weight: float32 [2048, 4096], P('fs', 'tp')
- new_copy: bfloat16 [2048, 4096], P('fs', 'tp')
All inputs are finite; a program needn't handle non-finite values.
Results may differ from a plain program's by a relative error of at most 0.006.
Values may be sent and summed in bfloat16 or wider, within the bound.
A program may use at most 64 MiB of HBM per device.

v0:
```python
import jax
import jax.numpy as jnp
from jax import lax
from jax.sharding import PartitionSpec as P

D = 2048
E = 4096


first_decay = 0.9
second_decay = 0.9
learn_rate = 0.05
epsilon = 1e-08


def on_device(saved_input, value_cotangent, factor, weight, first_moment, second_moment):
    factor_wide = factor.astype(jnp.float32)
    factor_whole = lax.all_gather(factor, "fs", axis=0, tiled=True)
    projected = jnp.dot(saved_input, factor_whole, preferred_element_type=jnp.float32)
    upper = projected.astype(jnp.bfloat16)
    lower = (projected - upper.astype(jnp.float32)).astype(jnp.bfloat16)
    dims = (((0,), (0,)), ((), ()))
    high_part = lax.dot_general(upper, value_cotangent, dims, preferred_element_type=jnp.float32)
    low_part = lax.dot_general(lower, value_cotangent, dims, preferred_element_type=jnp.float32)
    low_grad = lax.psum_scatter(high_part + low_part, "fs", scatter_dimension=0, tiled=True)
    low_grad = lax.psum(low_grad, "rep")
    new_first = first_decay * first_moment + (1.0 - first_decay) * low_grad
    new_second = second_decay * second_moment + (1.0 - second_decay) * low_grad * low_grad
    ratio = new_first / (jnp.sqrt(new_second) + epsilon)
    ratio_whole = lax.all_gather(ratio, "fs", axis=0, tiled=True)
    raw = jnp.dot(factor_wide, ratio_whole, precision=lax.Precision.HIGHEST)
    total = lax.psum(jnp.sum(raw * raw), ("fs", "tp"))
    spread = jnp.sqrt(total / (D * E))
    direction = raw / (spread + 1.0)
    new_weight = weight - learn_rate * direction
    return (low_grad, new_first, new_second, direction, new_weight, new_weight.astype(jnp.bfloat16))


def solution(mesh):
    placed = (
        P(("fs", "rep"), None),
        P(("fs", "rep"), "tp"),
        P("fs", None),
        P("fs", "tp"),
        P("fs", "tp"),
        P("fs", "tp"),
    )
    return jax.shard_map(
        on_device,
        mesh=mesh,
        in_specs=placed,
        out_specs=(
            P("fs", "tp"),
            P("fs", "tp"),
            P("fs", "tp"),
            P("fs", "tp"),
            P("fs", "tp"),
            P("fs", "tp"),
        ),
        check_vma=False,
    )
```

profile of v0, /device:TPU:0, one launch (start us, length us, event | category | flops | bytes accessed | tf_op | source)
XLA Modules:
  0.0 185.3 jit_solution(11213346444921834174)
XLA Ops:
  7.2 0.0 reduce-scatter.2.cloned.1.call-start
  7.2 0.0 copy-start
  7.2 17.7 %all_gather.6 = bf16[2048,128]{1,0:T(8,128)(2,1)S(1)} all-gather(bf16[512,128]{1,0:T(8,128)(2,1)} %param.8), channel_id=1, replica_groups=mesh['fs'=4,'rep'=4,'tp'=2] {'fs'}, dimensions={0}, use_global_device_ids=true | all-gather | bytes 655360 | tf_op jit(solution)/shard_map/all_gather | solution.py:18
  24.9 3.4 %fusion.6 = f32[1024,128]{1,0:T(8,128)S(1)} fusion(bf16[1024,2048]{1,0:T(8,128)(2,1)} %param.6, bf16[2048,128]{1,0:T(8,128)(2,1)S(1)} %all_gather.6), kind=kOutput, calls=%fused_computation.13 | convolution fusion | flops 536870912 | bytes 5242880 | tf_op jit(solution)/shard_map/dot_general | solution.py:19
  28.4 0.0 copy-done
  28.4 0.7 fusion.2
  29.1 0.0 copy-start.3
  29.1 0.0 copy-start.4
  29.2 1.7 convolution_add_fusion
  30.9 0.0 reduce-scatter.2.cloned.1.call-update
  30.9 0.0 all-reduce.2.cloned.1.call-start
  31.0 29.2 %reduce-scatter.2.cloned.1.call-done = f32[32,2048]{1,0:T(8,128)} async-done(((f32[128,2048]{1,0:T(8,128)}), f32[32,2048]{1,0:T(8,128)}) %reduce-scatter.2.cloned.1.call-update) | async-done | bytes 262160 | tf_op jit(solution)/shard_map/reduce_scatter | solution.py:25
  60.1 0.0 all-reduce.2.cloned.1.call-update
  60.1 0.0 all-gather.2.cloned.1.call-start
  60.2 44.5 %all-reduce.2.cloned.1.call-done = f32[32,2048]{1,0:T(8,128)} async-done(((f32[32,2048]{1,0:T(8,128)}), f32[32,2048]{1,0:T(8,128)}) %all-reduce.2.cloned.1.call-update) | async-done | bytes 262160 | tf_op jit(solution)/shard_map/psum | solution.py:26
  104.6 0.0 copy-done.3
  104.6 0.0 copy-done.4
  104.6 1.9 %add_divide_fusion = (f32[32,2048]{1,0:T(8,128)}, f32[32,2048]{1,0:T(8,128)}, f32[32,2048]{1,0:T(8,128)}) fusion(f32[32,2048]{1,0:T(8,128)} %all-reduce.2.cloned.1.call-done, f32[32,2048]{1,0:T(8,128)S(1)} %copy-done.3, f32[32,2048]{1,0:T(8,128)S(1)} %copy-done.4), kind=kLoop, calls=%fused_computation.8 | loop fusion | flops 524288 | bytes 1572864 | tf_op jit(solution)/shard_map/div | solution.py:29
  106.5 0.0 all-gather.2.cloned.1.call-update
  106.6 0.0 copy-start.2
  106.6 5.4 %copy.12 = f32[512,2048]{0,1:T(8,128)} copy(f32[512,2048]{1,0:T(8,128)} %param.9) | data formatting | bytes 8388608 | tf_op args[3]
  112.0 22.8 %all-gather.2.cloned.1.call-done = f32[128,2048]{1,0:T(8,128)} async-done(((f32[32,2048]{1,0:T(8,128)}), f32[128,2048]{1,0:T(8,128)}) %all-gather.2.cloned.1.call-update) | async-done | bytes 1048592 | tf_op jit(solution)/shard_map/all_gather | solution.py:30
  134.8 0.0 copy-done.2
  134.8 6.0 %multiply_reduce_fusion = (f32[]{:T(128)}, f32[2048,512]{1,0:T(8,128)}) fusion(f32[128,2048]{1,0:T(8,128)} %all-gather.2.cloned.1.call-done, bf16[512,128]{1,0:T(8,128)(2,1)S(1)} %copy-done.2), kind=kOutput, calls=%fused_computation.2 | convolution fusion | flops 1612709888 | bytes 5373956 | tf_op jit(solution)/shard_map/dot_general | solution.py:31
  140.8 15.3 %psum.15 = f32[]{:T(128)} all-reduce(f32[]{:T(128)} %get-tuple-element.18), channel_id=1, replica_groups=mesh['fs'=4,'rep'=4,'tp'=2] {'fs','tp'}, use_global_device_ids=true, to_apply=%region_3.0 | all-reduce | flops 1 | bytes 8 | tf_op jit(solution)/shard_map/psum | solution.py:32
  156.7 8.3 %fusion.4 = (bf16[512,2048]{0,1:T(8,128)(2,1)S(1)}, f32[512,2048]{0,1:T(8,128)}, f32[512,2048]{0,1:T(8,128)}) fusion(f32[512,2048]{0,1:T(8,128)} %copy.12, f32[2048,512]{1,0:T(8,128)} %get-tuple-element.19, f32[]{:T(128)S(6)} %add.29), kind=kLoop, calls=%fused_computation.12 | loop fusion | flops 4194304 | bytes 18874372 | tf_op jit(solution)/shard_map/convert_element_type | solution.py:36
  165.0 2.4 %copy.15 = bf16[512,2048]{1,0:T(8,128)(2,1)} copy(bf16[512,2048]{0,1:T(8,128)(2,1)S(1)} %get-tuple-element.12) | data formatting | bytes 4194304
  167.4 5.3 %copy.14 = f32[512,2048]{1,0:T(8,128)} copy(f32[512,2048]{0,1:T(8,128)} %get-tuple-element.13) | data formatting | bytes 8388608
  172.7 0.0 copy-start.1
  172.7 5.4 %copy.13 = f32[512,2048]{1,0:T(8,128)} copy(f32[512,2048]{0,1:T(8,128)} %get-tuple-element.14) | data formatting | bytes 8388608
  178.1 0.0 copy-done.1
  178.1 0.7 copy.17
Async XLA Ops:
  7.2 52.9 %reduce-scatter.2.cloned.1.call-start = ((), (), s32[]{:S(2)}) async-start(), calls=%async_computation.1 | async-start | bytes 1310720 | tf_op jit(solution)/shard_map/reduce_scatter | solution.py:25
  7.2 21.2 %copy-start = (bf16[1024,2048]{1,0:T(8,128)(2,1)S(1)}, bf16[1024,2048]{1,0:T(8,128)(2,1)}, u32[]{:S(2)}) copy-start(bf16[1024,2048]{1,0:T(8,128)(2,1)} %param.7) | copy-start | bytes 12582916
  29.1 75.5 %copy-start.3 = (f32[32,2048]{1,0:T(8,128)S(1)}, f32[32,2048]{1,0:T(8,128)}, u32[]{:S(2)}) copy-start(f32[32,2048]{1,0:T(8,128)} %param.11) | copy-start | bytes 786436
  29.1 75.5 %copy-start.4 = (f32[32,2048]{1,0:T(8,128)S(1)}, f32[32,2048]{1,0:T(8,128)}, u32[]{:S(2)}) copy-start(f32[32,2048]{1,0:T(8,128)} %param.10) | copy-start | bytes 786436
  30.9 73.7 %all-reduce.2.cloned.1.call-start = ((), (), s32[]{:S(2)}) async-start(), calls=%async_computation.2 | async-start | bytes 524288 | tf_op jit(solution)/shard_map/psum | solution.py:26
  60.1 74.7 %all-gather.2.cloned.1.call-start = ((), (), s32[]{:S(2)}) async-start(), calls=%async_computation.3 | async-start | bytes 1310720 | tf_op jit(solution)/shard_map/all_gather | solution.py:30
  106.6 28.2 %copy-start.2 = (bf16[512,128]{1,0:T(8,128)(2,1)S(1)}, bf16[512,128]{1,0:T(8,128)(2,1)}, u32[]{:S(2)}) copy-start(bf16[512,128]{1,0:T(8,128)(2,1)} %param.8) | copy-start | bytes 393220
  172.7 5.4 %copy-start.1 = (f32[32,2048]{1,0:T(8,128)S(1)}, f32[32,2048]{1,0:T(8,128)}, u32[]{:S(2)}) copy-start(f32[32,2048]{1,0:T(8,128)} %all-reduce.2.cloned.1.call-done) | copy-start | bytes 786436
Sparse Core Ops, SparseCore 0:
  31.0 29.0 reduce-scatter.1
  63.0 41.5 all-reduce.1
  106.8 27.9 all-gather.1
where the time goes:
time: 186 us; the launch traced here: 185 us
  waiting for transfers between devices  96.5 us (52%)
  blocking collectives  33 us (18%)
  local copies, waits for them, and re-layouts  19.2 us (10%)
  between operations  14.5 us (8%)
  matrix products  11.9 us (6%)
  other arithmetic  10.2 us (5%)
    psum x1, waiting for transfers between devices, on_device(): low_grad = lax.psum(low_grad, 'rep')  44.5 us
    reduce_scatter x1, waiting for transfers between devices, on_device(): lax.psum_scatter(high_part + low_part, 'fs', scatter_dimension=0, tiled=T...  29.2 us
    all_gather x1, waiting for transfers between devices, on_device(): ratio_whole = lax.all_gather(ratio, 'fs', axis=0, tiled=True)  22.8 us
    unnamed x15, local copies, waits for them, and re-layouts  19.2 us
    all_gather x1, blocking collectives, on_device(): factor_whole = lax.all_gather(factor, 'fs', axis=0, tiled=True)  17.7 us
    psum x1, blocking collectives, on_device(): total = lax.psum(jnp.sum(raw * raw), ('fs', 'tp'))  15.3 us
    convert_element_type x1, other arithmetic, on_device(): new_weight.astype(jnp.bfloat16)  8.28 us
    dot_general x1, matrix products, on_device(): raw = jnp.dot(factor_wide, ratio_whole, precision=lax.Precision.HIGHEST)  5.95 us
  transfers between devices with their start and end apart: 3, of which 3 were waited for; matrix products, arithmetic and copies ran while one was open for 3% of the time, Pallas kernels for 0%

commit v1 on v0

v1 whole, which is shorter than its diff:
```python
import functools

import jax
import jax.numpy as jnp
from jax import lax
from jax.experimental import pallas as pl
from jax.experimental.pallas import tpu as pltpu
from jax.sharding import PartitionSpec as P

first_decay = 0.9
second_decay = 0.9
learn_rate = 0.05
epsilon = 1e-08

CHUNKS = 2
TILE = 64
MESH = pl.DeviceIdType.MESH


def moved(src, dst, send, recv, where):
    return pltpu.make_async_remote_copy(
        src_ref=src, dst_ref=dst, send_sem=send, recv_sem=recv, device_id=where, device_id_type=MESH
    )


def merged(ref, count, rows):
    if rows % 16 == 0:
        block = ref[...]
        return block.reshape(count * rows, block.shape[-1])
    pieces = [ref[i].astype(jnp.float32) for i in range(count)]
    return jnp.concatenate(pieces, axis=0).astype(jnp.bfloat16)


def exchange(
    nfs, nrep, ntp, entries,
    x_hbm, v_hbm, f_hbm, m1_hbm, m2_hbm,
    ratio_out, low_out, scale_out,
    x, v, m1, m2, fall, proj, pt, gram,
    own1, send1, recv1, own2, send2, recv2, low_own, low_all, rgat, rall, sc_send, sc_recv,
    local_sem, fs_send, fs_recv, fd_send, fd_recv, s1_send, s1_recv, s2_send, s2_recv,
    a1_send, a1_recv, a2_send, a2_recv, lg_send, lg_recv, t_send, t_recv,
):
    f, r, c = lax.axis_index("fs"), lax.axis_index("rep"), lax.axis_index("tp")
    hr = fall.shape[2]
    rank, cw = own1.shape[1], own1.shape[2]
    block = cw * CHUNKS
    rp = rank // nfs
    f32, bf16 = jnp.float32, jnp.bfloat16

    locals_ = [
        pltpu.make_async_copy(f_hbm.at[pl.ds(0, hr)], fall.at[f, 0], local_sem.at[0]),
        pltpu.make_async_copy(f_hbm.at[pl.ds(hr, hr)], fall.at[f, 1], local_sem.at[1]),
        pltpu.make_async_copy(x_hbm, x, local_sem.at[2]),
        pltpu.make_async_copy(v_hbm, v, local_sem.at[3]),
        pltpu.make_async_copy(m1_hbm, m1, local_sem.at[4]),
        pltpu.make_async_copy(m2_hbm, m2, local_sem.at[5]),
    ]
    for copy in locals_:
        copy.start()

    barrier = pltpu.get_barrier_semaphore()
    for e in range(1, nfs):
        pl.semaphore_signal(barrier, inc=1, device_id={"fs": lax.rem(f + e, nfs)}, device_id_type=MESH)
    for d in range(1, nrep):
        pl.semaphore_signal(barrier, inc=1, device_id={"rep": lax.rem(r + d, nrep)}, device_id_type=MESH)
    other = {"tp": 1 - c}
    pl.semaphore_signal(barrier, inc=1, device_id=other, device_id_type=MESH)
    pl.semaphore_wait(barrier, nfs + nrep - 1)

    sends = []

    fcopies, dcopies = [], []
    for e in range(1, nfs):
        copy = moved(
            f_hbm.at[pl.ds(c * hr, hr)], fall.at[f, c], fs_send.at[e - 1], fs_recv.at[e - 1],
            {"fs": lax.rem(f + e, nfs)},
        )
        copy.start()
        fcopies.append(copy)
        sends.append(copy)
    incremental = (2 * hr) % 128 == 0

    def project(src, first):
        piece = fall[src].reshape(2 * hr, fall.shape[3])
        cols = pl.ds(pl.multiple_of(src * (2 * hr), 128), 2 * hr)
        term = jnp.dot(x[:, cols], piece, preferred_element_type=f32)
        if first:
            proj[...] = term
        else:
            proj[...] += term

    locals_[0].wait()
    locals_[1].wait()
    locals_[2].wait()
    if incremental:
        project(f, True)
    for e in range(1, nfs + 1):
        if e < nfs:
            src = lax.rem(f - e + nfs, nfs)
            fcopies[e - 1].wait_recv()
            copy = moved(fall.at[src, c], fall.at[src, c], fd_send.at[e - 1], fd_recv.at[e - 1], other)
            copy.start()
            dcopies.append(copy)
            sends.append(copy)
        if e > 1:
            dcopies[e - 2].wait_recv()
            if incremental:
                project(lax.rem(f - (e - 1) + nfs, nfs), False)
    if not incremental:
        whole = fall[...].reshape(nfs * 2 * hr, fall.shape[3])
        proj[...] = jnp.dot(x[...], whole, preferred_element_type=f32)

    turned = proj[...].T
    upper = turned.astype(bf16)
    pt[:rank] = upper
    pt[rank:] = (turned - upper.astype(f32)).astype(bf16)

    locals_[3].wait()
    copies1 = {}
    for q in range(CHUNKS):
        for d in list(range(1, nrep)) + [0]:
            to = lax.rem(r + d, nrep)
            cols = pl.ds(pl.multiple_of(to * block + q * cw, 128), cw)
            both = jnp.dot(pt[...], v[:, cols], preferred_element_type=f32)
            term = both[:rank] + both[rank:]
            if d == 0:
                own1[q] = term
            else:
                send1[q, d - 1] = term.astype(bf16)
                copy = moved(
                    send1.at[q, d - 1], recv1.at[q, d - 1], s1_send.at[q, d - 1], s1_recv.at[q, d - 1],
                    {"rep": to},
                )
                copy.start()
                copies1[q, d] = copy
                sends.append(copy)

    whole = fall[...].reshape(nfs * 2 * hr, fall.shape[3])
    square = lax.dot_general(whole, whole, (((0,), (0,)), ((), ())), preferred_element_type=f32)
    upper = square.astype(bf16)
    gram[:rank] = upper
    gram[rank:] = (square - upper.astype(f32)).astype(bf16)
    locals_[4].wait()
    locals_[5].wait()

    copies2 = {}
    for q in range(CHUNKS):
        total = own1[q]
        for d in range(1, nrep):
            copies1[q, d].wait_recv()
            total = total + recv1[q, d - 1].astype(f32)
        for i in range(nfs):
            part = total[i * rp:(i + 1) * rp]
            own2[q, i] = part
            send2[q, i] = part.astype(bf16)
        for e in range(1, nfs):
            to = lax.rem(f + e, nfs)
            copy = moved(
                send2.at[q, to], recv2.at[q, e - 1], s2_send.at[q, e - 1], s2_recv.at[q, e - 1], {"fs": to}
            )
            copy.start()
            copies2[q, e] = copy
            sends.append(copy)

    copies3, low_copies = {}, []
    for q in range(CHUNKS):
        low = own2[q, f]
        for e in range(1, nfs):
            copies2[q, e].wait_recv()
            low = low + recv2[q, e - 1].astype(f32)
        cols = pl.ds(pl.multiple_of(r * block + q * cw, 128), cw)
        new_first = first_decay * m1[:, cols] + (1.0 - first_decay) * low
        new_second = second_decay * m2[:, cols] + (1.0 - second_decay) * low * low
        ratio = new_first / (jnp.sqrt(new_second) + epsilon)
        rgat[q, f] = ratio.astype(bf16)
        low_own[q] = low
        for e in range(1, nfs):
            copy = moved(
                rgat.at[q, f], rgat.at[q, f], a1_send.at[q, e - 1], a1_recv.at[q, e - 1],
                {"fs": lax.rem(f + e, nfs)},
            )
            copy.start()
            copies3[q, e] = copy
            sends.append(copy)
        for d in range(1, nrep):
            copy = moved(
                low_own.at[q], low_all.at[q, d - 1], lg_send.at[q, d - 1], lg_recv.at[q, d - 1],
                {"rep": lax.rem(r + d, nrep)},
            )
            copy.start()
            low_copies.append((q, d, copy))
            sends.append(copy)

    squares = jnp.zeros((1, 1), f32)

    def place(piece, owner, q):
        cols = pl.ds(pl.multiple_of(owner * block + q * cw, 128), cw)
        ratio_out[:, cols] = piece
        both = jnp.dot(gram[...], piece, preferred_element_type=f32)
        terms = (both[:rank] + both[rank:]) * piece.astype(f32)
        return jnp.sum(jnp.sum(terms, axis=0, keepdims=True), axis=1, keepdims=True)

    copies4 = {}
    for q in range(CHUNKS):
        for e in range(1, nfs):
            copies3[q, e].wait_recv()
        for d in range(1, nrep):
            copy = moved(
                rgat.at[q], rall.at[q, d - 1], a2_send.at[q, d - 1], a2_recv.at[q, d - 1],
                {"rep": lax.rem(r + d, nrep)},
            )
            copy.start()
            copies4[q, d] = copy
            sends.append(copy)
        squares = squares + place(merged(rgat.at[q], nfs, rp), r, q)
        cols = pl.ds(pl.multiple_of(r * block + q * cw, 128), cw)
        low_out[:, cols] = low_own[q]

    for q, d, copy in low_copies:
        copy.wait_recv()
        owner = lax.rem(r - d + nrep, nrep)
        low_out[:, pl.ds(pl.multiple_of(owner * block + q * cw, 128), cw)] = low_all[q, d - 1]

    for q in range(CHUNKS):
        for d in range(1, nrep):
            copies4[q, d].wait_recv()
            piece = merged(rall.at[q, d - 1], nfs, rp)
            squares = squares + place(piece, lax.rem(r - d + nrep, nrep), q)

    sc_send[...] = jnp.broadcast_to(squares, sc_send.shape)
    copy = moved(sc_send, sc_recv, t_send, t_recv, other)
    copy.start()
    sends.append(copy)
    copy.wait_recv()
    spread = jnp.sqrt((sc_send[...] + sc_recv[...]) / entries)
    scale_out[...] = 1.0 / (spread + 1.0)
    for copy in sends:
        copy.wait_send()


def update(factor, ratio, scale, low, m1, m2, weight, low_out, first_out, second_out, dir_out, weight_out, copy_out):
    @pl.when(pl.program_id(0) == 0)
    def _():
        grad = low[...]
        low_out[...] = grad
        first_out[...] = first_decay * m1[...] + (1.0 - first_decay) * grad
        second_out[...] = second_decay * m2[...] + (1.0 - second_decay) * grad * grad

    raw = jnp.dot(factor[...], ratio[...], preferred_element_type=jnp.float32)
    direction = raw * scale[0:1, 0:1]
    dir_out[...] = direction
    new_weight = weight[...] - learn_rate * direction
    weight_out[...] = new_weight
    copy_out[...] = new_weight.astype(jnp.bfloat16)


def on_device(nfs, nrep, ntp, saved_input, value_cotangent, factor, weight, first_moment, second_moment):
    f32, bf16 = jnp.float32, jnp.bfloat16
    tokens, width = saved_input.shape
    cols = value_cotangent.shape[1]
    rows, rank = factor.shape
    rp = rank // nfs
    cw = cols // nrep // CHUNKS
    hr = rows // 2
    any_spec = pl.BlockSpec(memory_space=pl.ANY)
    vmem = pl.BlockSpec(memory_space=pltpu.VMEM)
    dma = pltpu.SemaphoreType.DMA
    V = pltpu.VMEM
    pf, pr = nfs - 1, nrep - 1
    ratio, low, scale = pl.pallas_call(
        functools.partial(exchange, nfs, nrep, ntp, float(width) * cols * ntp),
        out_shape=(
            jax.ShapeDtypeStruct((rank, cols), bf16),
            jax.ShapeDtypeStruct((rp, cols), f32),
            jax.ShapeDtypeStruct((8, 128), f32),
        ),
        in_specs=[any_spec] * 5,
        out_specs=(vmem, vmem, vmem),
        scratch_shapes=[
            V((tokens, width), bf16),
            V((tokens, cols), bf16),
            V((rp, cols), f32),
            V((rp, cols), f32),
            V((nfs, 2, hr, rank), bf16),
            V((tokens, rank), f32),
            V((2 * rank, tokens), bf16),
            V((2 * rank, rank), bf16),
            V((CHUNKS, rank, cw), f32),
            V((CHUNKS, pr, rank, cw), bf16),
            V((CHUNKS, pr, rank, cw), bf16),
            V((CHUNKS, nfs, rp, cw), f32),
            V((CHUNKS, nfs, rp, cw), bf16),
            V((CHUNKS, pf, rp, cw), bf16),
            V((CHUNKS, rp, cw), f32),
            V((CHUNKS, pr, rp, cw), f32),
            V((CHUNKS, nfs, rp, cw), bf16),
            V((CHUNKS, pr, nfs, rp, cw), bf16),
            V((8, 128), f32),
            V((8, 128), f32),
            dma((6,)),
            dma((pf,)), dma((pf,)), dma((pf,)), dma((pf,)),
            dma((CHUNKS, pr)), dma((CHUNKS, pr)),
            dma((CHUNKS, pf)), dma((CHUNKS, pf)),
            dma((CHUNKS, pf)), dma((CHUNKS, pf)),
            dma((CHUNKS, pr)), dma((CHUNKS, pr)),
            dma((CHUNKS, pr)), dma((CHUNKS, pr)),
            dma, dma,
        ],
        compiler_params=pltpu.CompilerParams(
            collective_id=0, has_side_effects=True, vmem_limit_bytes=40 * 1024 * 1024
        ),
        name="exchange",
    )(saved_input, value_cotangent, factor, first_moment, second_moment)

    tile = min(TILE, rows)
    fixed = lambda shape: pl.BlockSpec(shape, lambda i: (0, 0))
    moving = lambda shape: pl.BlockSpec(shape, lambda i: (i, 0))
    return pl.pallas_call(
        update,
        grid=(rows // tile,),
        out_shape=(
            jax.ShapeDtypeStruct((rp, cols), f32),
            jax.ShapeDtypeStruct((rp, cols), f32),
            jax.ShapeDtypeStruct((rp, cols), f32),
            jax.ShapeDtypeStruct((rows, cols), f32),
            jax.ShapeDtypeStruct((rows, cols), f32),
            jax.ShapeDtypeStruct((rows, cols), bf16),
        ),
        in_specs=[
            moving((tile, rank)),
            fixed((rank, cols)),
            fixed((8, 128)),
            fixed((rp, cols)),
            fixed((rp, cols)),
            fixed((rp, cols)),
            moving((tile, cols)),
        ],
        out_specs=(
            fixed((rp, cols)), fixed((rp, cols)), fixed((rp, cols)),
            moving((tile, cols)), moving((tile, cols)), moving((tile, cols)),
        ),
        name="update",
    )(factor, ratio, scale, low, first_moment, second_moment, weight)


def solution(mesh):
    placed = (
        P(("fs", "rep"), None),
        P(("fs", "rep"), "tp"),
        P("fs", None),
        P("fs", "tp"),
        P("fs", "tp"),
        P("fs", "tp"),
    )
    sizes = mesh.shape
    return jax.shard_map(
        functools.partial(on_device, sizes["fs"], sizes["rep"], sizes["tp"]),
        mesh=mesh,
        in_specs=placed,
        out_specs=(P("fs", "tp"),) * 6,
        check_vma=False,
    )
```

time: 186 us -> 57.8 us (0.31)
  waiting for transfers between devices: 96.5 us -> 0 us
  Pallas kernels: 0 us -> 47.5 us
  blocking collectives: 33 us -> 0 us
  between operations: 14.5 us -> 0.66 us
  matrix products: 11.9 us -> 0 us
  other arithmetic: 10.2 us -> 0 us
  local copies, waits for them, and re-layouts: 19.2 us -> 9.26 us
    pallas_call x0 -> x2, Pallas kernels: none -> 47.5 us  [the longest x1 38.6 us: on_device(): pl.pallas_call(functools.partial(exchange, nfs, nrep, ntp, float(width) *...]
    psum x1 -> x0, waiting for transfers between devices: 44.5 us -> none  [on_device(): low_grad = lax.psum(low_grad, 'rep')]
    reduce_scatter x1 -> x0, waiting for transfers between devices: 29.2 us -> none  [on_device(): lax.psum_scatter(high_part + low_part, 'fs', scatter_dimension=0, tiled=T...]
    all_gather x1 -> x0, waiting for transfers between devices: 22.8 us -> none  [on_device(): ratio_whole = lax.all_gather(ratio, 'fs', axis=0, tiled=True)]
    all_gather x1 -> x0, blocking collectives: 17.7 us -> none  [on_device(): factor_whole = lax.all_gather(factor, 'fs', axis=0, tiled=True)]
    psum x1 -> x0, blocking collectives: 15.3 us -> none  [on_device(): total = lax.psum(jnp.sum(raw * raw), ('fs', 'tp'))]
    dot_general x4 -> x0, matrix products: 11.9 us -> none  [the longest x1 5.95 us: on_device(): raw = jnp.dot(factor_wide, ratio_whole, precision=lax.Precision.HIGHEST)]
    unnamed x15 -> x16, local copies, waits for them, and re-layouts: 19.2 us -> 9.26 us
  transfers between devices with their start and end apart: 3 -> 0, of which waited for: 3 -> 0; matrix products, arithmetic and copies ran while one was open for 3% -> 0% of each run, Pallas kernels for 0% -> 0%
where the time goes in v1:
time: 57.8 us; the launch traced here: 57.4 us
  Pallas kernels  47.5 us (82%)
  local copies, waits for them, and re-layouts  9.26 us (16%)
  between operations  0.66 us (1%)
    pallas_call x1, Pallas kernels, on_device(): pl.pallas_call(functools.partial(exchange, nfs, nrep, ntp, float(width) *...  38.6 us
    unnamed x16, local copies, waits for them, and re-layouts  9.26 us
    pallas_call x1, Pallas kernels, on_device(): pl.pallas_call(update, grid=(rows // tile,), out_shape=(jax.ShapeDtypeStr...  8.89 us

profile of v1, /device:TPU:0, one launch (start us, length us, event | category | flops | bytes accessed | tf_op | source)
XLA Modules:
  0.0 57.4 jit_solution(13944811851251267249)
XLA Ops:
  0.6 0.0 copy-start
  0.6 2.2 %copy-done = bf16[1024,2048]{1,0:T(8,128)(2,1)S(1)} copy-done((bf16[1024,2048]{1,0:T(8,128)(2,1)S(1)}, bf16[1024,2048]{1,0:T(8,128)(2,1)}, u32[]{:S(2)}) %copy-start) | copy-done | bytes 4194328
  2.8 0.0 copy-start.1
  2.8 2.2 %copy-done.1 = bf16[1024,2048]{1,0:T(8,128)(2,1)S(1)} copy-done((bf16[1024,2048]{1,0:T(8,128)(2,1)S(1)}, bf16[1024,2048]{1,0:T(8,128)(2,1)}, u32[]{:S(2)}) %copy-start.1) | copy-done | bytes 4194328
  5.0 0.0 copy-start.2
  5.0 0.9 %copy-done.2 = f32[32,2048]{1,0:T(8,128)S(1)} copy-done((f32[32,2048]{1,0:T(8,128)S(1)}, f32[32,2048]{1,0:T(8,128)}, u32[]{:S(2)}) %copy-start.2) | copy-done | bytes 262168
  6.0 0.0 copy-start.3
  6.0 0.9 %copy-done.3 = f32[32,2048]{1,0:T(8,128)S(1)} copy-done((f32[32,2048]{1,0:T(8,128)S(1)}, f32[32,2048]{1,0:T(8,128)}, u32[]{:S(2)}) %copy-start.3) | copy-done | bytes 262168
  6.9 0.0 copy-start.4
  6.9 0.9 %copy-done.4 = bf16[512,128]{1,0:T(8,128)(2,1)S(1)} copy-done((bf16[512,128]{1,0:T(8,128)(2,1)S(1)}, bf16[512,128]{1,0:T(8,128)(2,1)}, u32[]{:S(2)}) %copy-start.4) | copy-done | bytes 131096
  7.8 38.6 %exchange.1 = (bf16[128,2048]{1,0:T(8,128)(2,1)S(1)}, f32[32,2048]{1,0:T(8,128)S(1)}, f32[8,128]{1,0:T(8,128)S(1)}) custom-call(bf16[1024,2048]{1,0:T(8,128)(2,1)S(1)} %copy-done, bf16[1024,2048]{1,0:T(8,128)(2,1)S(1)} %copy-done.1, bf16[512,128]{1,0:T(8,128)(2,1)S(1)} %copy-done.4, f32[32,2048]{1,0:T(8,128)S(1)} %copy-done.2, f32[32,2048]{1,0:T(8,128)S(1)} %copy-done.3), custom_call_target="tpu_custom_call" | custom-call | tf_op jit(solution)/shard_map/exchange/pallas_call | solution.py:270
  46.4 0.0 copy-start.5
  46.4 0.8 %copy-done.5 = bf16[128,2048]{1,0:T(8,128)(2,1)} copy-done((bf16[128,2048]{1,0:T(8,128)(2,1)}, bf16[128,2048]{1,0:T(8,128)(2,1)S(1)}, u32[]{:S(2)}) %copy-start.5) | copy-done | bytes 524312
  47.2 0.0 copy-start.6
  47.2 0.7 %copy-done.6 = f32[32,2048]{1,0:T(8,128)} copy-done((f32[32,2048]{1,0:T(8,128)}, f32[32,2048]{1,0:T(8,128)S(1)}, u32[]{:S(2)}) %copy-start.6) | copy-done | bytes 262168
  47.9 0.0 copy-start.7
  47.9 0.6 %copy-done.7 = f32[8,128]{1,0:T(8,128)} copy-done((f32[8,128]{1,0:T(8,128)}, f32[8,128]{1,0:T(8,128)S(1)}, u32[]{:S(2)}) %copy-start.7) | copy-done | bytes 4120
  48.5 8.9 %update.1 = (f32[32,2048]{1,0:T(8,128)}, f32[32,2048]{1,0:T(8,128)}, f32[32,2048]{1,0:T(8,128)}, f32[512,2048]{1,0:T(8,128)}, f32[512,2048]{1,0:T(8,128)}, /*index=5*/bf16[512,2048]{1,0:T(8,128)(2,1)}) custom-call(bf16[512,128]{1,0:T(8,128)(2,1)} %factor.1, bf16[128,2048]{1,0:T(8,128)(2,1)} %copy-done.5, f32[8,128]{1,0:T(8,128)} %copy-done.7, ...), custom_call_target="tpu_custom_call" | custom-call | tf_op jit(solution)/shard_map/update/pallas_call | solution.py:318
Async XLA Ops:
  0.6 2.2 %copy-start = (bf16[1024,2048]{1,0:T(8,128)(2,1)S(1)}, bf16[1024,2048]{1,0:T(8,128)(2,1)}, u32[]{:S(2)}) copy-start(bf16[1024,2048]{1,0:T(8,128)(2,1)} %x_hbm.1) | copy-start | bytes 12582916
  2.8 2.2 %copy-start.1 = (bf16[1024,2048]{1,0:T(8,128)(2,1)S(1)}, bf16[1024,2048]{1,0:T(8,128)(2,1)}, u32[]{:S(2)}) copy-start(bf16[1024,2048]{1,0:T(8,128)(2,1)} %v_hbm.1) | copy-start | bytes 12582916
  5.0 0.9 %copy-start.2 = (f32[32,2048]{1,0:T(8,128)S(1)}, f32[32,2048]{1,0:T(8,128)}, u32[]{:S(2)}) copy-start(f32[32,2048]{1,0:T(8,128)} %m1.1) | copy-start | bytes 786436
  6.0 0.9 %copy-start.3 = (f32[32,2048]{1,0:T(8,128)S(1)}, f32[32,2048]{1,0:T(8,128)}, u32[]{:S(2)}) copy-start(f32[32,2048]{1,0:T(8,128)} %m2.1) | copy-start | bytes 786436
  6.9 0.9 %copy-start.4 = (bf16[512,128]{1,0:T(8,128)(2,1)S(1)}, bf16[512,128]{1,0:T(8,128)(2,1)}, u32[]{:S(2)}) copy-start(bf16[512,128]{1,0:T(8,128)(2,1)} %factor.1) | copy-start | bytes 393220
  46.4 0.8 %copy-start.5 = (bf16[128,2048]{1,0:T(8,128)(2,1)}, bf16[128,2048]{1,0:T(8,128)(2,1)S(1)}, u32[]{:S(2)}) copy-start(bf16[128,2048]{1,0:T(8,128)(2,1)S(1)} %get-tuple-element.9.ratio) | copy-start | bytes 1572868
  47.2 0.7 %copy-start.6 = (f32[32,2048]{1,0:T(8,128)}, f32[32,2048]{1,0:T(8,128)S(1)}, u32[]{:S(2)}) copy-start(f32[32,2048]{1,0:T(8,128)S(1)} %get-tuple-element.11.low) | copy-start | bytes 786436
  47.9 0.6 %copy-start.7 = (f32[8,128]{1,0:T(8,128)}, f32[8,128]{1,0:T(8,128)S(1)}, u32[]{:S(2)}) copy-start(f32[8,128]{1,0:T(8,128)S(1)} %get-tuple-element.10.scale) | copy-start | bytes 12292
